TPU v7x, 512 devices: a whole 4x4x16 slice. The times are simulated.
512 devices in a mesh: fs: 64 (over z, y), tp: 8 (over x, core).
Axes of the slice: x: 4, y: 4, z: 16, core: 2. Of those that a mesh axis runs over, the one named last changes fastest.
Arguments:
- tokens: bfloat16 [16384, 2048], P('fs'), may hold values from -6 to 6
- mix_gain: float32 [2048], replicated, may hold values from 0.1 to 1.9
- glu_value: bfloat16 [2048, 2048], P('fs', 'tp'), may hold values from -0.125 to 0.125
- glu_gate: bfloat16 [2048, 2048], P('fs', 'tp'), may hold values from -0.125 to 0.125
- conv_taps: float32 [31, 2048], P(None, 'tp'), may hold values from -2.2 to 2.2, as said below
- chan_gain: float32 [2048], P('tp'), may hold values from 0.1 to 1.9
- mix_out: bfloat16 [2048, 2048], P('tp', 'fs'), may hold values from -0.125 to 0.125
- mlp_gain: float32 [2048], replicated, may hold values from 0.1 to 1.9
- up_weight: bfloat16 [2048, 8192], P('fs', 'tp'), may hold values from -0.125 to 0.125
- down_weight: bfloat16 [8192, 2048], P('tp', 'fs'), may hold values from -0.0625 to 0.0625
Outputs:
- result: bfloat16 [16384, 2048], P('fs')
Inputs may be any that keep to these rules, and one draw needn't show every extreme that they name: `conv_taps`: independent entries scaled by fan-in; channels fall into 16 groups of different scale.
All inputs are finite; a program needn't handle non-finite values.
Results may differ from a plain program's by a relative error of at most 0.018.
Values may be sent and summed in bfloat16 or wider, within the bound.
A program may use at most 64 MiB of HBM per device.

v0:
```python
import jax
import jax.numpy as jnp
from jax import lax
from jax.sharding import PartitionSpec as P

C = 2048
LEN = 128
norm_floor = 0.05


def in_one_piece(arrays, axis, dim, along):
    widths = [a.shape[along] for a in arrays]
    both = jnp.concatenate(arrays, axis=along)
    result = lax.all_gather(both, axis, axis=dim, tiled=True)
    return tuple(jnp.split(result, [sum(widths[:k]) for k in range(1, len(widths))], axis=along))


def rows_first(arrays, axis, dims):
    turned = [jnp.moveaxis(a, dim, 0) for a, dim in zip(arrays, dims)]
    both = jnp.concatenate([t.reshape(len(t), -1) for t in turned], axis=1)
    result, at, gathered = (lax.all_gather(both, axis, axis=0, tiled=True), 0, [])
    for t, dim in zip(turned, dims):
        piece = result[:, at : at + t[0].size].reshape(-1, *t.shape[1:])
        gathered.append(jnp.moveaxis(piece, 0, dim))
        at += t[0].size
    return tuple(gathered)


def sent_to_all(shard, axis):
    count = lax.axis_size(axis)
    return lax.all_to_all(
        jnp.broadcast_to(shard[None], (count, *shard.shape)), axis, 0, 0, tiled=True
    )


def over_copies(shard, axis):
    everything = sent_to_all(shard, axis)
    return jnp.sum(everything, axis=0)


def together(arrays, axis):
    vector, at, gathered = (jnp.concatenate([a.reshape(-1) for a in arrays]), 0, [])
    running = over_copies(vector, axis)
    for a in arrays:
        gathered.append(running[at : at + a.size].reshape(a.shape))
        at += a.size
    return tuple(gathered)


def in_blocks(shard, dim, count):
    shape = shard.shape
    pieces = shard.reshape(*shape[:dim], count, shape[dim] // count, *shape[dim + 1 :])
    return jnp.moveaxis(pieces, dim, 0)


def summed_on_arrival(shard, axis, dim):
    count = lax.axis_size(axis)
    pieces = lax.all_to_all(in_blocks(shard, dim, count), axis, 0, 0, tiled=True)
    return jnp.sum(pieces.astype(jnp.float32), axis=0)


def joined_along(pieces, dim):
    shape = list(pieces.shape[1:])
    shape[dim] *= pieces.shape[0]
    return jnp.moveaxis(pieces, 0, dim).reshape(shape)


def gather_directly(shard, axis, dim):
    return joined_along(sent_to_all(shard, axis), dim)


def rms_scale(stream, gain):
    return stream * lax.rsqrt(jnp.mean(stream * stream, axis=-1, keepdims=True) + norm_floor) * gain


def bf16_round(value):
    return lax.optimization_barrier(value.astype(jnp.bfloat16)).astype(jnp.float32)


def depthwise(glu, conv_taps):
    seqs = glu.shape[0] // LEN
    blocks = glu.reshape(seqs, LEN, glu.shape[1]).astype(jnp.float32)
    reach = conv_taps.shape[0] // 2
    padded = jnp.pad(blocks, ((0, 0), (reach, reach), (0, 0)))
    total = jnp.zeros_like(blocks)
    for offset in range(conv_taps.shape[0]):
        total = total + padded[:, offset : offset + LEN] * conv_taps[offset]
    return total.reshape(glu.shape)


def per_device(
    tokens,
    mix_gain,
    glu_value,
    glu_gate,
    conv_taps,
    chan_gain,
    mix_out,
    mlp_gain,
    up_weight,
    down_weight,
):
    stream = tokens.astype(jnp.float32)
    normed = rms_scale(stream, mix_gain).astype(jnp.bfloat16)
    row_parts = in_one_piece((glu_value, glu_gate, up_weight), "fs", 0, 1)
    column_parts = rows_first((mix_out, down_weight), "fs", (1, 1))
    values = jnp.dot(normed, row_parts[0], preferred_element_type=jnp.float32)
    gating = jnp.dot(normed, row_parts[1], preferred_element_type=jnp.float32)
    glu = (values * jax.nn.sigmoid(gating)).astype(jnp.bfloat16)
    convolved = depthwise(glu, conv_taps)
    sums, squares = together(
        (jnp.sum(convolved, axis=-1), jnp.sum(convolved * convolved, axis=-1)), "tp"
    )
    centre = (sums / C)[:, None]
    spread = (squares / C)[:, None] - centre * centre
    hidden = jax.nn.silu((convolved - centre) * lax.rsqrt(spread + norm_floor) * chan_gain).astype(
        jnp.bfloat16
    )
    whole_out = column_parts[0]
    own_rows = stream.shape[0] // lax.axis_size("tp")
    mixed = summed_on_arrival(
        jnp.dot(hidden, whole_out, preferred_element_type=jnp.float32).astype(jnp.bfloat16), "tp", 0
    )
    own_stream = lax.dynamic_slice_in_dim(stream, lax.axis_index("tp") * own_rows, own_rows, 0)
    resid = own_stream + bf16_round(mixed)
    normed_mlp = rms_scale(resid, mlp_gain).astype(jnp.bfloat16)
    whole_up = row_parts[2]
    active = jnp.square(
        jax.nn.relu(
            jnp.dot(
                gather_directly(normed_mlp, "tp", 0), whole_up, preferred_element_type=jnp.float32
            )
        )
    ).astype(jnp.bfloat16)
    whole_down = column_parts[1]
    feed = summed_on_arrival(
        jnp.dot(active, whole_down, preferred_element_type=jnp.float32).astype(jnp.bfloat16),
        "tp",
        0,
    )
    finished = (resid + bf16_round(feed)).astype(jnp.bfloat16)
    return gather_directly(finished, "tp", 0)


def solution(mesh):
    in_specs = (
        P("fs", None),
        P(),
        P("fs", "tp"),
        P("fs", "tp"),
        P(None, "tp"),
        P("tp"),
        P("tp", "fs"),
        P(),
        P("fs", "tp"),
        P("tp", "fs"),
    )
    out_specs = P("fs", None)
    return jax.shard_map(
        per_device, mesh=mesh, in_specs=in_specs, out_specs=out_specs, check_vma=False
    )
```

profile of v0, /device:TPU:1, one launch (start us, length us, event | category | flops | bytes accessed | tf_op | source)
XLA Modules:
  0.0 408.4 jit_solution(4157544092094613481)
XLA Ops:
  6.5 1.5 pad_maximum_fusion
  8.1 1.5 pad_maximum_fusion.1
  9.6 1.5 multiply_reduce_fusion
  11.2 1.0 fusion.94
  12.1 1.0 fusion.93
  13.2 145.1 %all-gather.3.cloned.1.call-done = bf16[2048,1536]{1,0:T(8,128)(2,1)} async-done(((bf16[32,1536]{1,0:T(8,128)(2,1)}), bf16[2048,1536]{1,0:T(8,128)(2,1)}) %all-gather.3.cloned.1.call-update) | async-done | bytes 6291472 | tf_op jit(solution)/shard_map/all_gather | solution.py:14
  158.3 2.0 fusion.23
  160.4 1.8 bitcast_convert_fusion
  162.1 1.2 fusion.91
  163.3 17.4 %all_to_all.26 = f32[8,1,512]{2,1,0:T(1,128)S(1)} all-to-all(f32[8,1,512]{2,1,0:T(1,128)S(1)} %broadcast_in_dim.6), channel_id=1, replica_groups=mesh['fs'=64,'tp'=8] {'tp'}, dimensions={0} | all-to-all | bytes 32768 | tf_op jit(solution)/shard_map/all_to_all | solution.py:31
  180.8 0.2 multiply_convert_fusion.4
  181.0 123.2 %all-gather.5.cloned.1.call-done = bf16[2048,1280]{1,0:T(8,128)(2,1)} async-done(((bf16[32,1280]{1,0:T(8,128)(2,1)}), bf16[2048,1280]{1,0:T(8,128)(2,1)}) %all-gather.5.cloned.1.call-update) | async-done | bytes 5242896 | tf_op jit(solution)/shard_map/all_gather | solution.py:21
  304.2 2.7 convolution_convert_fusion
  306.9 14.1 %all-to-all-start.1 = ((bf16[8,32,2048]{2,1,0:T(8,128)(2,1)}), bf16[8,32,2048]{2,1,0:T(8,128)(2,1)S(1)}, u32[]{:S(2)}, u32[]{:S(2)}) async-start(bf16[8,32,2048]{2,1,0:T(8,128)(2,1)} %bitcast.38), calls=%async_computation.1 | async-start | bytes 2097152 | tf_op jit(solution)/shard_map/all_to_all | solution.py:58
  320.9 1.7 convert_element_type.45
  322.6 13.3 %all-to-all-done.1 = bf16[8,32,2048]{2,1,0:T(8,128)(2,1)S(1)} async-done(((bf16[8,32,2048]{2,1,0:T(8,128)(2,1)}), bf16[8,32,2048]{2,1,0:T(8,128)(2,1)S(1)}, u32[]{:S(2)}, u32[]{:S(2)}) %all-to-all-start.1) | async-done | bytes 1048608 | tf_op jit(solution)/shard_map/all_to_all | solution.py:58
  336.1 1.1 multiply_reduce_fusion.1
  337.2 1.0 multiply_convert_fusion.3
  338.4 18.3 %all_to_all.27 = bf16[8,32,2048]{2,1,0:T(8,128)(2,1)S(1)} all-to-all(bf16[8,32,2048]{2,1,0:T(8,128)(2,1)S(1)} %broadcast_in_dim.7), channel_id=1, replica_groups=mesh['fs'=64,'tp'=8] {'tp'}, dimensions={0} | all-to-all | bytes 2097152 | tf_op jit(solution)/shard_map/all_to_all | solution.py:31
  356.7 5.8 %fusion.4 = bf16[256,2048]{1,0:T(8,128)(2,1)S(1)} fusion(bf16[2048,1280]{1,0:T(8,128)(2,1)} %all-gather.5.cloned.1.call-done, bf16[256,2048]{1,0:T(8,128)(2,1)S(1)} %bitcast.53, bf16[2048,1536]{1,0:T(8,128)(2,1)} %all-gather.3.cloned.1.call-done), kind=kOutput, calls=%fused_computation.4 | convolution fusion | flops 2148794368 | bytes 10485760 | tf_op jit(solution)/shard_map/dot_general | solution.py:137
  362.5 18.4 %all_to_all.28 = bf16[8,32,2048]{2,1,0:T(8,128)(2,1)S(1)} all-to-all(bf16[8,32,2048]{2,1,0:T(8,128)(2,1)S(1)} %bitcast.54), channel_id=1, replica_groups=mesh['fs'=64,'tp'=8] {'tp'}, dimensions={0} | all-to-all | bytes 2097152 | tf_op jit(solution)/shard_map/all_to_all | solution.py:58
  381.0 1.0 add_convert_fusion
  382.2 18.4 %all_to_all.29 = bf16[8,32,2048]{2,1,0:T(8,128)(2,1)S(1)} all-to-all(bf16[8,32,2048]{2,1,0:T(8,128)(2,1)S(1)} %broadcast_in_dim.8), channel_id=1, replica_groups=mesh['fs'=64,'tp'=8] {'tp'}, dimensions={0} | all-to-all | bytes 2097152 | tf_op jit(solution)/shard_map/all_to_all | solution.py:31
  400.6 1.0 copy.16
  (22 shorter events, 0.7 us)
Async XLA Ops:
  6.5 151.8 %all-gather.3.cloned.1.call-start = ((), (), s32[]{:S(2)}) async-start(), calls=%async_computation.5 | async-start | bytes 6389760 | tf_op jit(solution)/shard_map/all_gather | solution.py:14
  8.1 296.2 %all-gather.5.cloned.1.call-start = ((), (), s32[]{:S(2)}) async-start(), calls=%async_computation.6 | async-start | bytes 5324800 | tf_op jit(solution)/shard_map/all_gather | solution.py:21
  11.1 149.2 %copy-start = (bf16[256,2048]{1,0:T(8,128)(2,1)S(1)}, bf16[256,2048]{1,0:T(8,128)(2,1)}, u32[]{:S(2)}) copy-start(bf16[256,2048]{1,0:T(8,128)(2,1)} %param.10) | copy-start | bytes 3145732
  11.1 149.2 %copy-start.3 = (f32[2048]{0:T(1024)S(1)}, f32[2048]{0:T(1024)}, u32[]{:S(2)}) copy-start(f32[2048]{0:T(1024)} %param.11) | copy-start | bytes 24580
  160.4 20.4 %copy-start.2 = (f32[256]{0:T(256)S(1)}, f32[256]{0:T(256)}, u32[]{:S(2)}) copy-start(f32[256]{0:T(256)} %param.15) | copy-start | bytes 3076
  306.9 29.0 %all-to-all-start.1 = ((bf16[8,32,2048]{2,1,0:T(8,128)(2,1)}), bf16[8,32,2048]{2,1,0:T(8,128)(2,1)S(1)}, u32[]{:S(2)}, u32[]{:S(2)}) async-start(bf16[8,32,2048]{2,1,0:T(8,128)(2,1)} %bitcast.38), calls=%async_computation.1 | async-start | bytes 2097152 | tf_op jit(solution)/shard_map/all_to_all | solution.py:58
  320.9 16.2 %copy-start.1 = (f32[2048]{0:T(1024)S(1)}, f32[2048]{0:T(1024)}, u32[]{:S(2)}) copy-start(f32[2048]{0:T(1024)} %param.17) | copy-start | bytes 24580
Sparse Core Ops, SparseCore 0:
  10.3 147.9 all-gather.2
  161.2 142.9 all-gather.4
where the time goes:
time: 409 us; the launch traced here: 408 us
  waiting for transfers between devices  282 us (69%)
  blocking collectives  72.5 us (18%)
  starting transfers between devices  14.1 us (3%)
  between operations  13.5 us (3%)
  matrix products  12.3 us (3%)
  other arithmetic  11 us (3%)
    all_gather x1, waiting for transfers between devices, in_one_piece(): result = lax.all_gather(both, axis, axis=dim, tiled=True)  145 us
    all_gather x1, waiting for transfers between devices, rows_first(): lax.all_gather(both, axis, axis=0, tiled=True)  123 us
    all_to_all x3, blocking collectives, sent_to_all(): lax.all_to_all(jnp.broadcast_to(shard[None], (count, *shard.shape)), axis...  54.1 us
    all_to_all x1, blocking collectives, summed_on_arrival(): lax.all_to_all(in_blocks(shard, dim, count), axis, 0, 0, tiled=True)  18.4 us
    all_to_all x1, starting transfers between devices, summed_on_arrival(): lax.all_to_all(in_blocks(shard, dim, count), axis, 0, 0, tiled=True)  14.1 us
    all_to_all x1, waiting for transfers between devices, summed_on_arrival(): lax.all_to_all(in_blocks(shard, dim, count), axis, 0, 0, tiled=True)  13.3 us
  transfers between devices with their start and end apart: 3, of which 3 were waited for; matrix products, arithmetic and copies ran while one was open for 3% of the time, Pallas kernels for 0%

commit v1 on v0

--- a/solution.py
+++ b/solution.py
@@ -6,6 +6,11 @@
 C = 2048
 LEN = 128
 norm_floor = 0.05
+
+
+def exchange_gather(x, axis, along):
+    outgoing = jnp.stack([x] * lax.axis_size(axis))
+    return jnp.concatenate(lax.all_to_all(outgoing, axis, 0, 0), axis=along)
 
 
 def in_one_piece(arrays, axis, dim, along):
@@ -18,7 +23,7 @@
 def rows_first(arrays, axis, dims):
     turned = [jnp.moveaxis(a, dim, 0) for a, dim in zip(arrays, dims)]
     both = jnp.concatenate([t.reshape(len(t), -1) for t in turned], axis=1)
-    result, at, gathered = (lax.all_gather(both, axis, axis=0, tiled=True), 0, [])
+    result, at, gathered = (exchange_gather(both, axis, 0), 0, [])
     for t, dim in zip(turned, dims):
         piece = result[:, at : at + t[0].size].reshape(-1, *t.shape[1:])
         gathered.append(jnp.moveaxis(piece, 0, dim))

time: 409 us -> 524 us (1.28)
  waiting for transfers between devices: 282 us -> 391 us
  starting transfers between devices: 14.1 us -> 35 us
  blocking collectives: 72.5 us -> 55.1 us
    all_to_all x0 -> x2, waiting for transfers between devices: none -> 231 us  [the longest x1 227 us: exchange_gather(): return jnp.concatenate(lax.all_to_all(outgoing, axis, 0, 0), axis=along)]
    all_gather x1 -> x0, waiting for transfers between devices: 123 us -> none  [rows_first(): lax.all_gather(both, axis, axis=0, tiled=True)]
    all_to_all x0 -> x2, starting transfers between devices: none -> 22.7 us  [the longest x1 13 us: sent_to_all(): lax.all_to_all(jnp.broadcast_to(shard[None], (count, *shard.shape)), axis...]
    all_to_all x3 -> x2, blocking collectives: 54.1 us -> 36.7 us  [sent_to_all(): lax.all_to_all(jnp.broadcast_to(shard[None], (count, *shard.shape)), axis...]
  transfers between devices with their start and end apart: 3 -> 4, of which waited for: 3 -> 4; matrix products, arithmetic and copies ran while one was open for 3% -> 1% of each run, Pallas kernels for 0% -> 0%
where the time goes in v1:
time: 524 us
  waiting for transfers between devices  391 us (75%)
  blocking collectives  55.1 us (11%)
  starting transfers between devices  35 us (7%)
  between operations  13.5 us (3%)
  matrix products  12.3 us (2%)
  other arithmetic  9.66 us (2%)
  local copies, waits for them, and re-layouts  6.74 us (1%)
    all_to_all x1, waiting for transfers between devices, exchange_gather(): return jnp.concatenate(lax.all_to_all(outgoing, axis, 0, 0), axis=along)  227 us
    all_gather x1, waiting for transfers between devices, in_one_piece(): result = lax.all_gather(both, axis, axis=dim, tiled=True)  147 us
    all_to_all x2, blocking collectives, sent_to_all(): lax.all_to_all(jnp.broadcast_to(shard[None], (count, *shard.shape)), axis...  36.7 us
    all_to_all x1, blocking collectives, summed_on_arrival(): lax.all_to_all(in_blocks(shard, dim, count), axis, 0, 0, tiled=True)  18.4 us
    all_to_all x1, waiting for transfers between devices, summed_on_arrival(): lax.all_to_all(in_blocks(shard, dim, count), axis, 0, 0, tiled=True)  13.3 us
    all_to_all x1, starting transfers between devices, sent_to_all(): lax.all_to_all(jnp.broadcast_to(shard[None], (count, *shard.shape)), axis...  13 us
    all_to_all x1, starting transfers between devices, summed_on_arrival(): lax.all_to_all(in_blocks(shard, dim, count), axis, 0, 0, tiled=True)  12.3 us
  transfers between devices with their start and end apart: 4, of which 4 were waited for; matrix products, arithmetic and copies ran while one was open for 1% of the time, Pallas kernels for 0%

profile of v1, /device:TPU:1, one launch (start us, length us, event | category | flops | bytes accessed | tf_op | source)
XLA Modules:
  0.0 523.7 jit_solution(14273237429983482215)
XLA Ops:
  6.5 1.6 pad_maximum_fusion
  8.1 1.5 multiply_reduce_fusion
  9.7 1.0 fusion.94
  10.6 1.0 fusion.93
  11.7 146.6 %all-gather.2.cloned.1.call-done = bf16[2048,1536]{1,0:T(8,128)(2,1)} async-done(((bf16[32,1536]{1,0:T(8,128)(2,1)}), bf16[2048,1536]{1,0:T(8,128)(2,1)}) %all-gather.2.cloned.1.call-update) | async-done | bytes 6291472 | tf_op jit(solution)/shard_map/all_gather | solution.py:19
  158.3 2.0 fusion.23
  160.4 1.7 bitcast_convert_fusion
  162.1 1.2 fusion.91
  163.9 13.0 %all-to-all-start = ((f32[8,1,512]{2,1,0:T(1,128)}), f32[8,1,512]{2,1,0:T(1,128)S(1)}, u32[]{:S(2)}, u32[]{:S(2)}) async-start(f32[8,1,512]{2,1,0:T(1,128)} %broadcast_in_dim.6), calls=%async_computation | async-start | bytes 32768 | tf_op jit(solution)/shard_map/all_to_all | solution.py:36
  176.9 4.6 all-to-all-done
  181.6 2.9 stack.2
  184.5 9.7 %all-to-all-start.1 = ((bf16[64,32,1280]{2,1,0:T(8,128)(2,1)}), bf16[64,32,1280]{2,1,0:T(8,128)(2,1)}, u32[]{:S(2)}, u32[]{:S(2)}) async-start(bf16[64,32,1280]{2,1,0:T(8,128)(2,1)} %stack.2), calls=%async_computation.1 | async-start | bytes 10485760 | tf_op jit(solution)/shard_map/all_to_all | solution.py:13
  194.4 226.8 %all-to-all-done.1 = bf16[64,32,1280]{2,1,0:T(8,128)(2,1)} async-done(((bf16[64,32,1280]{2,1,0:T(8,128)(2,1)}), bf16[64,32,1280]{2,1,0:T(8,128)(2,1)}, u32[]{:S(2)}, u32[]{:S(2)}) %all-to-all-start.1) | async-done | bytes 5242912 | tf_op jit(solution)/shard_map/all_to_all | solution.py:13
  421.2 2.7 convolution_convert_fusion
  423.9 12.3 %all-to-all-start.2 = ((bf16[8,32,2048]{2,1,0:T(8,128)(2,1)}), bf16[8,32,2048]{2,1,0:T(8,128)(2,1)S(1)}, u32[]{:S(2)}, u32[]{:S(2)}) async-start(bf16[8,32,2048]{2,1,0:T(8,128)(2,1)} %bitcast.39), calls=%async_computation.2 | async-start | bytes 2097152 | tf_op jit(solution)/shard_map/all_to_all | solution.py:63
  436.2 1.7 convert_element_type.45
  437.9 13.3 %all-to-all-done.2 = bf16[8,32,2048]{2,1,0:T(8,128)(2,1)S(1)} async-done(((bf16[8,32,2048]{2,1,0:T(8,128)(2,1)}), bf16[8,32,2048]{2,1,0:T(8,128)(2,1)S(1)}, u32[]{:S(2)}, u32[]{:S(2)}) %all-to-all-start.2) | async-done | bytes 1048608 | tf_op jit(solution)/shard_map/all_to_all | solution.py:63
  451.4 1.1 multiply_reduce_fusion.1
  452.5 1.1 multiply_convert_fusion.3
  453.7 18.3 %all_to_all.31 = bf16[8,32,2048]{2,1,0:T(8,128)(2,1)S(1)} all-to-all(bf16[8,32,2048]{2,1,0:T(8,128)(2,1)S(1)} %broadcast_in_dim.7), channel_id=1, replica_groups=mesh['fs'=64,'tp'=8] {'tp'}, dimensions={0} | all-to-all | bytes 2097152 | tf_op jit(solution)/shard_map/all_to_all | solution.py:36
  472.0 5.8 %fusion.4 = bf16[256,2048]{1,0:T(8,128)(2,1)S(1)} fusion(bf16[2048,1280]{1,0:T(8,128)(2,1)} %bitcast.38, bf16[256,2048]{1,0:T(8,128)(2,1)S(1)} %bitcast.54, bf16[2048,1536]{1,0:T(8,128)(2,1)} %all-gather.2.cloned.1.call-done), kind=kOutput, calls=%fused_computation.4 | convolution fusion | flops 2148794368 | bytes 10485760 | tf_op jit(solution)/shard_map/dot_general | solution.py:142
  477.8 18.4 %all_to_all.32 = bf16[8,32,2048]{2,1,0:T(8,128)(2,1)S(1)} all-to-all(bf16[8,32,2048]{2,1,0:T(8,128)(2,1)S(1)} %bitcast.55), channel_id=1, replica_groups=mesh['fs'=64,'tp'=8] {'tp'}, dimensions={0} | all-to-all | bytes 2097152 | tf_op jit(solution)/shard_map/all_to_all | solution.py:63
  496.4 1.0 add_convert_fusion
  497.5 18.4 %all_to_all.33 = bf16[8,32,2048]{2,1,0:T(8,128)(2,1)S(1)} all-to-all(bf16[8,32,2048]{2,1,0:T(8,128)(2,1)S(1)} %broadcast_in_dim.8), channel_id=1, replica_groups=mesh['fs'=64,'tp'=8] {'tp'}, dimensions={0} | all-to-all | bytes 2097152 | tf_op jit(solution)/shard_map/all_to_all | solution.py:36
  (27 shorter events, 2.4 us)
Async XLA Ops:
  6.5 153.8 %copy-start = (bf16[256,2048]{1,0:T(8,128)(2,1)S(1)}, bf16[256,2048]{1,0:T(8,128)(2,1)}, u32[]{:S(2)}) copy-start(bf16[256,2048]{1,0:T(8,128)(2,1)} %param.10) | copy-start | bytes 3145732
  6.5 153.8 %copy-start.5 = (f32[2048]{0:T(1024)S(1)}, f32[2048]{0:T(1024)}, u32[]{:S(2)}) copy-start(f32[2048]{0:T(1024)} %param.11) | copy-start | bytes 24580
  6.5 151.8 %all-gather.2.cloned.1.call-start = ((), (), s32[]{:S(2)}) async-start(), calls=%async_computation.6 | async-start | bytes 6389760 | tf_op jit(solution)/shard_map/all_gather | solution.py:19
  11.7 165.2 %copy-start.1 = (bf16[1024,32]{0,1:T(8,128)(2,1)S(1)}, bf16[1024,32]{0,1:T(8,128)(2,1)}, u32[]{:S(2)}) copy-start(bf16[1024,32]{0,1:T(8,128)(2,1)} %param.19) | copy-start | bytes 196612
  11.7 165.2 %copy-start.2 = (bf16[256,32]{0,1:T(8,128)(2,1)S(1)}, bf16[256,32]{0,1:T(8,128)(2,1)}, u32[]{:S(2)}) copy-start(bf16[256,32]{0,1:T(8,128)(2,1)} %param.16) | copy-start | bytes 49156
  163.9 17.6 %all-to-all-start = ((f32[8,1,512]{2,1,0:T(1,128)}), f32[8,1,512]{2,1,0:T(1,128)S(1)}, u32[]{:S(2)}, u32[]{:S(2)}) async-start(f32[8,1,512]{2,1,0:T(1,128)} %broadcast_in_dim.6), calls=%async_computation | async-start | bytes 32768 | tf_op jit(solution)/shard_map/all_to_all | solution.py:36
  184.5 9.8 %copy-start.4 = (f32[256]{0:T(256)S(1)}, f32[256]{0:T(256)}, u32[]{:S(2)}) copy-start(f32[256]{0:T(256)} %param.15) | copy-start | bytes 3076
  184.5 236.8 %all-to-all-start.1 = ((bf16[64,32,1280]{2,1,0:T(8,128)(2,1)}), bf16[64,32,1280]{2,1,0:T(8,128)(2,1)}, u32[]{:S(2)}, u32[]{:S(2)}) async-start(bf16[64,32,1280]{2,1,0:T(8,128)(2,1)} %stack.2), calls=%async_computation.1 | async-start | bytes 10485760 | tf_op jit(solution)/shard_map/all_to_all | solution.py:13
  421.2 31.3 %copy-start.3 = (f32[2048]{0:T(1024)S(1)}, f32[2048]{0:T(1024)}, u32[]{:S(2)}) copy-start(f32[2048]{0:T(1024)} %param.17) | copy-start | bytes 24580
  423.9 27.3 %all-to-all-start.2 = ((bf16[8,32,2048]{2,1,0:T(8,128)(2,1)}), bf16[8,32,2048]{2,1,0:T(8,128)(2,1)S(1)}, u32[]{:S(2)}, u32[]{:S(2)}) async-start(bf16[8,32,2048]{2,1,0:T(8,128)(2,1)} %bitcast.39), calls=%async_computation.2 | async-start | bytes 2097152 | tf_op jit(solution)/shard_map/all_to_all | solution.py:63
Sparse Core Ops, SparseCore 0:
  10.3 147.9 all-gather.1
